TPU v7x, 128 devices: a whole 4x4x4 slice. The times are simulated.
128 devices in a mesh: fs: 16 (over z, y), tp: 8 (over x, core).
Axes of the slice: x: 4, y: 4, z: 4, core: 2. Of those that a mesh axis runs over, the one named last changes fastest.
Arguments:
- normed_input: bfloat16 [24576, 2048], P(('fs', 'tp')), may hold values from -6 to 6
- pre_act: bfloat16 [24576, 8192], P('fs', 'tp'), may hold values from -6 to 6
- out_grad: bfloat16 [24576, 2048], P(('fs', 'tp')), may hold values from -24 to 24
- up_weight: bfloat16 [2048, 8192], P('fs', 'tp'), may hold values from -0.125 to 0.125
- down_weight: bfloat16 [8192, 2048], P('tp', 'fs'), may hold values from -0.0625 to 0.0625
Outputs:
- input_grad: bfloat16 [24576, 2048], P(('fs', 'tp'))
- up_grad: float32 [2048, 8192], P('fs', 'tp')
- down_grad: float32 [8192, 2048], P('tp', 'fs')
All inputs are finite; a program needn't handle non-finite values.
Results may differ from a plain program's by a relative error of at most 0.014.
Values may be sent and summed in bfloat16 or wider, within the bound.
A program may use at most 128 MiB of HBM per device.

v0:
```python
import jax
import jax.numpy as jnp
from jax import lax
from jax.sharding import PartitionSpec as P


def sent_together(arrays, axis, dim, along):
    ends, at = ([], 0)
    for a in arrays[:-1]:
        at += a.shape[along]
        ends.append(at)
    both = jnp.concatenate(arrays, axis=along)
    return tuple(jnp.split(lax.all_gather(both, axis, axis=dim, tiled=True), ends, axis=along))


def cut_along(x, dim, count):
    before, after = (x.shape[:dim], x.shape[dim + 1 :])
    return jnp.moveaxis(x.reshape(*before, count, -1, *after), dim, 0)


def sum_at_owner(x, axis, dim):
    tiles = cut_along(x, dim, lax.axis_size(axis))
    arrived = lax.all_to_all(tiles, axis, split_axis=0, concat_axis=0, tiled=True)
    return arrived.astype(jnp.float32).sum(axis=0)


def local(normed_input, pre_act, out_grad, up_weight, down_weight):
    rows_all, grad_rows = sent_together((normed_input, out_grad), "tp", 0, 1)
    active = jnp.maximum(pre_act.astype(jnp.float32), 0.0)
    hidden = (active * active).astype(jnp.bfloat16)
    width = pre_act.shape[1]
    columns = grad_rows
    hidden_grad = jnp.dot(
        columns,
        lax.all_gather(down_weight, "fs", axis=1, tiled=True).T,
        preferred_element_type=jnp.float32,
    )
    pre_grad = (2.0 * active * hidden_grad).astype(jnp.bfloat16)
    partial_value = jnp.dot(
        pre_grad,
        lax.all_gather(up_weight, "fs", axis=0, tiled=True).T,
        preferred_element_type=jnp.float32,
    )
    rounded = lax.optimization_barrier(partial_value.astype(jnp.bfloat16))
    summed = sum_at_owner(rounded.astype(jnp.float32).astype(jnp.bfloat16), "tp", 0)
    input_grad = summed.astype(jnp.bfloat16)
    columns = rows_all
    both = lax.psum_scatter(
        jnp.concatenate(
            [
                jnp.dot(columns.T, pre_grad, preferred_element_type=jnp.float32),
                jnp.dot(grad_rows.T, hidden, preferred_element_type=jnp.float32),
            ],
            axis=1,
        ).astype(jnp.bfloat16),
        "fs",
        scatter_dimension=0,
        tiled=True,
    ).astype(jnp.float32)
    up_grad = both[:, :width]
    down_grad = both[:, width:].T
    up_grad, down_grad = (up_grad, down_grad)
    return (input_grad, up_grad, down_grad)


def solution(mesh):
    placed = (
        P(("fs", "tp"), None),
        P("fs", "tp"),
        P(("fs", "tp"), None),
        P("fs", "tp"),
        P("tp", "fs"),
    )
    return jax.shard_map(
        local,
        mesh=mesh,
        in_specs=placed,
        out_specs=(P(("fs", "tp"), None), P("fs", "tp"), P("tp", "fs")),
        check_vma=False,
    )
```

profile of v0, /device:TPU:1, one launch (start us, length us, event | category | flops | bytes accessed | tf_op | source)
XLA Modules:
  0.0 293.3 jit_solution(11470290909760394026)
XLA Ops:
  7.2 0.0 all-gather.4.cloned.1.call-start
  7.2 2.7 pad_maximum_fusion.1
  9.9 0.0 all-gather.6.cloned.1.call-start
  10.0 0.7 all-gather.6.cloned.1.call-update
  10.7 0.0 all-gather.8.cloned.1.call-start
  10.7 0.7 all-gather.8.cloned.1.call-update
  11.4 0.0 reduce-scatter.4.cloned.1.call-start
  11.5 69.5 %all-gather.4.cloned.1.call-done = bf16[1536,4096]{1,0:T(8,128)(2,1)} async-done(((bf16[192,4096]{1,0:T(8,128)(2,1)}), bf16[1536,4096]{1,0:T(8,128)(2,1)}) %all-gather.4.cloned.1.call-update) | async-done | bytes 12582928 | tf_op jit(solution)/shard_map/all_gather | solution.py:13
  80.9 11.6 %fusion.8 = bf16[2048,1024]{0,1:T(8,128)(2,1)} fusion(bf16[1536,4096]{1,0:T(8,128)(2,1)} %all-gather.4.cloned.1.call-done, bf16[1536,1024]{1,0:T(8,128)(2,1)} %param.6), kind=kOutput, calls=%fused_computation.11 | convolution fusion | flops 6450839552 | bytes 13631488 | tf_op jit(solution)/shard_map/dot_general | solution.py:52
  92.6 46.1 %all-gather.6.cloned.1.call-done = bf16[1024,2048]{1,0:T(8,128)(2,1)} async-done(((bf16[1024,128]{1,0:T(8,128)(2,1)}), bf16[1024,2048]{1,0:T(8,128)(2,1)}) %all-gather.6.cloned.1.call-update) | async-done | bytes 4194320 | tf_op jit(solution)/shard_map/all_gather | solution.py:35
  138.7 10.3 %multiply_convert_fusion.1 = bf16[1536,1024]{1,0:T(8,128)(2,1)S(1)} fusion(bf16[1536,1024]{1,0:T(8,128)(2,1)S(1)} %copy-done.1, bf16[1024,2048]{1,0:T(8,128)(2,1)} %all-gather.6.cloned.1.call-done, bf16[1536,4096]{1,0:T(8,128)(2,1)} %all-gather.4.cloned.1.call-done), kind=kOutput, calls=%fused_computation.5 | convolution fusion | flops 6450315264 | bytes 16777216 | tf_op jit(solution)/shard_map/dot_general | solution.py:33
  149.0 1.7 copy-done.2
  150.7 8.4 %fusion.11 = bf16[2048,1024]{0,1:T(8,128)(2,1)} fusion(bf16[1536,1024]{1,0:T(8,128)(2,1)S(1)} %multiply_convert_fusion.1, bf16[1536,4096]{1,0:T(8,128)(2,1)S(1)} %copy-done), kind=kOutput, calls=%fused_computation.12 | convolution fusion | flops 6444548096 | bytes 13631488 | tf_op jit(solution)/shard_map/dot_general | solution.py:51
  159.1 8.4 %pad_maximum_fusion = bf16[2048,2048]{0,1:T(8,128)(2,1)} fusion(bf16[2048,1024]{0,1:T(8,128)(2,1)} %fusion.8, bf16[2048,1024]{0,1:T(8,128)(2,1)} %fusion.11), kind=kLoop, calls=%fused_computation | loop fusion | flops 16777216 | bytes 16777216 | tf_op jit(solution)/shard_map/concatenate | solution.py:49
  167.5 11.9 %copy.10 = bf16[2048,2048]{1,0:T(8,128)(2,1)} copy(bf16[2048,2048]{0,1:T(8,128)(2,1)} %pad_maximum_fusion) | data formatting | bytes 16777216
  179.4 0.0 reduce-scatter.4.cloned.1.call-update
  179.4 13.4 %all-gather.8.cloned.1.call-done = bf16[2048,1024]{1,0:T(8,128)(2,1)} async-done(((bf16[128,1024]{1,0:T(8,128)(2,1)}), bf16[2048,1024]{1,0:T(8,128)(2,1)}) %all-gather.8.cloned.1.call-update) | async-done | bytes 4194320 | tf_op jit(solution)/shard_map/all_gather | solution.py:41
  192.8 9.3 %convolution_convert_fusion = bf16[1536,2048]{1,0:T(8,128)(2,1)S(1)} fusion(bf16[1536,1024]{1,0:T(8,128)(2,1)S(1)} %copy-done.3, bf16[2048,1024]{1,0:T(8,128)(2,1)} %all-gather.8.cloned.1.call-done), kind=kOutput, calls=%fused_computation.1 | convolution fusion | flops 6445596672 | bytes 13631488 | tf_op jit(solution)/shard_map/dot_general | solution.py:39
  202.2 76.1 %all_to_all.5 = bf16[8,192,2048]{2,1,0:T(8,128)(2,1)} all-to-all(bf16[8,192,2048]{2,1,0:T(8,128)(2,1)S(1)} %bitcast.8), channel_id=1, replica_groups=mesh['fs'=16,'tp'=8] {'tp'}, dimensions={0} | all-to-all | bytes 12582912 | tf_op jit(solution)/shard_map/all_to_all | solution.py:23
  278.3 5.2 %reduce_sum.12 = bf16[192,2048]{1,0:T(8,128)(2,1)} reduce(bf16[8,192,2048]{2,1,0:T(8,128)(2,1)} %all_to_all.5, bf16[]{:T(256)} %constant.6.clone.1), dimensions={0}, to_apply=%region_0.0 | reduce | flops 2752512 | bytes 7077890 | tf_op jit(solution)/shard_map/reduce_sum | solution.py:24
  283.5 1.3 copy.11
  284.8 0.1 convert_element_type.24
  284.9 0.8 slice_bitcast_fusion
  285.8 1.0 copy.9
  (10 shorter events, 0.1 us)
Async XLA Ops:
  7.2 73.8 %all-gather.4.cloned.1.call-start = ((), (), s32[]{:S(2)}) async-start(), calls=%async_computation.2 | async-start | bytes 14155776 | tf_op jit(solution)/shard_map/all_gather | solution.py:13
  9.9 128.8 %all-gather.6.cloned.1.call-start = ((), (), s32[]{:S(2)}) async-start(), calls=%async_computation.3 | async-start | bytes 4456448 | tf_op jit(solution)/shard_map/all_gather | solution.py:35
  10.7 182.1 %all-gather.8.cloned.1.call-start = ((), (), s32[]{:S(2)}) async-start(), calls=%async_computation.4 | async-start | bytes 4456448 | tf_op jit(solution)/shard_map/all_gather | solution.py:41
  11.4 127.3 %copy-start.1 = (bf16[1536,1024]{1,0:T(8,128)(2,1)S(1)}, bf16[1536,1024]{1,0:T(8,128)(2,1)}, u32[]{:S(2)}) copy-start(bf16[1536,1024]{1,0:T(8,128)(2,1)} %param.6) | copy-start | bytes 9437188
  11.4 272.0 %reduce-scatter.4.cloned.1.call-start = ((), (), s32[]{:S(2)}) async-start(), calls=%async_computation.5 | async-start | bytes 8912896
  138.7 12.0 %copy-start = (bf16[1536,4096]{1,0:T(8,128)(2,1)S(1)}, bf16[1536,4096]{1,0:T(8,128)(2,1)}, u32[]{:S(2)}) copy-start(bf16[1536,4096]{1,0:T(8,128)(2,1)} %all-gather.4.cloned.1.call-done) | copy-start | bytes 37748740
  149.0 1.7 copy-start.2
  179.4 13.4 %copy-start.3 = (bf16[1536,1024]{1,0:T(8,128)(2,1)S(1)}, bf16[1536,1024]{1,0:T(8,128)(2,1)}, u32[]{:S(2)}) copy-start(bf16[1536,1024]{1,0:T(8,128)(2,1)} %copy-done.2) | copy-start | bytes 9437188
Sparse Core Ops, SparseCore 0:
  10.1 70.8 all-gather.3
  83.0 55.6 all-gather.5
  140.8 51.9 all-gather.7
  196.1 84.5 reduce-scatter.3
where the time goes:
time: 294 us; the launch traced here: 293 us
  waiting for transfers between devices  130 us (44%)
  blocking collectives  76.1 us (26%)
  matrix products  39.6 us (13%)
  local copies, waits for them, and re-layouts  16.8 us (6%)
  other arithmetic  16.4 us (6%)
  between operations  13.8 us (5%)
    all_to_all x1, blocking collectives, sum_at_owner(): lax.all_to_all(tiles, axis, split_axis=0, concat_axis=0, tiled=True)  76.1 us
    all_gather x1, waiting for transfers between devices, sent_together(): lax.all_gather(both, axis, axis=dim, tiled=True)  69.5 us
    all_gather x1, waiting for transfers between devices, local(): lax.all_gather(down_weight, 'fs', axis=1, tiled=True)  46.1 us
    unnamed x11, local copies, waits for them, and re-layouts  15.9 us
    all_gather x1, waiting for transfers between devices, local(): lax.all_gather(up_weight, 'fs', axis=0, tiled=True)  13.4 us
    dot_general x1, matrix products, local(): jnp.dot(grad_rows.T, hidden, preferred_element_type=jnp.float32)  11.6 us
    dot_general x1, matrix products, local(): jnp.dot(columns, lax.all_gather(down_weight, 'fs', axis=1, tiled=True).T,...  10.3 us
    dot_general x1, matrix products, local(): jnp.dot(pre_grad, lax.all_gather(up_weight, 'fs', axis=0, tiled=True).T,...  9.33 us
  transfers between devices with their start and end apart: 4, of which 3 were waited for; matrix products, arithmetic and copies ran while one was open for 22% of the time, Pallas kernels for 0%

commit v1 on v0

--- a/solution.py
+++ b/solution.py
@@ -2,6 +2,24 @@
 import jax.numpy as jnp
 from jax import lax
 from jax.sharding import PartitionSpec as P
+
+
+def gather_around(array, axis, dim):
+    ways, here, step = (lax.axis_size(axis), lax.axis_index(axis), array.shape[dim])
+    shape = [n * ways if d == dim else n for d, n in enumerate(array.shape)]
+    full = lax.dynamic_update_slice_in_dim(
+        jnp.zeros(shape, array.dtype), array, here * step, axis=dim
+    )
+    going_up = going_down = array
+    for far in range(1, ways // 2 + 1):
+        going_up = lax.ppermute(going_up, axis, [(d, (d + 1) % ways) for d in range(ways)])
+        full = lax.dynamic_update_slice_in_dim(full, going_up, (here - far) % ways * step, axis=dim)
+        if 2 * far < ways:
+            going_down = lax.ppermute(going_down, axis, [(d, (d - 1) % ways) for d in range(ways)])
+            full = lax.dynamic_update_slice_in_dim(
+                full, going_down, (here + far) % ways * step, axis=dim
+            )
+    return full
 
 
 def sent_together(arrays, axis, dim, along):
@@ -31,9 +49,7 @@
     width = pre_act.shape[1]
     columns = grad_rows
     hidden_grad = jnp.dot(
-        columns,
-        lax.all_gather(down_weight, "fs", axis=1, tiled=True).T,
-        preferred_element_type=jnp.float32,
+        columns, gather_around(down_weight, "fs", 1).T, preferred_element_type=jnp.float32
     )
     pre_grad = (2.0 * active * hidden_grad).astype(jnp.bfloat16)
     partial_value = jnp.dot(

time: 294 us -> 249 us (0.85)
  waiting for transfers between devices: 130 us -> 25.2 us
  starting transfers between devices: 0.16 us -> 37.3 us
  local copies, waits for them, and re-layouts: 16.8 us -> 33.8 us
  blocking collectives: 76.1 us -> 83.4 us
    all_gather x1, waiting for transfers between devices: 69.5 us -> 0.01 us  [sent_together(): lax.all_gather(both, axis, axis=dim, tiled=True)]
    all_gather x1 -> x0, waiting for transfers between devices: 46.1 us -> none  [local(): lax.all_gather(down_weight, 'fs', axis=1, tiled=True)]
    ppermute x0 -> x15, starting transfers between devices: none -> 37.2 us  [the longest x7 35 us: gather_around(): lax.ppermute(going_down, axis, [(d, (d - 1) % ways) for d in range(ways)])]
    ppermute x0 -> x15, waiting for transfers between devices: none -> 25.2 us  [the longest x8 20.8 us: gather_around(): lax.ppermute(going_up, axis, [(d, (d + 1) % ways) for d in range(ways)])]
    all_gather x1, waiting for transfers between devices: 13.4 us -> 0.02 us  [local(): lax.all_gather(up_weight, 'fs', axis=0, tiled=True)]
    dynamic_update_slice x0 -> x16, local copies, waits for them, and re-layouts: none -> 12.3 us  [the longest x8 6.11 us: gather_around(): lax.dynamic_update_slice_in_dim(full, going_up, (here - far) % ways * ste...]
    all_to_all x1, blocking collectives: 76.1 us -> 83.4 us  [sum_at_owner(): lax.all_to_all(tiles, axis, split_axis=0, concat_axis=0, tiled=True)]
    unnamed x11 -> x13, local copies, waits for them, and re-layouts: 15.9 us -> 18.2 us
  transfers between devices with their start and end apart: 4 -> 18, of which waited for: 3 -> 8; matrix products, arithmetic and copies ran while one was open for 22% -> 32% of each run, Pallas kernels for 0% -> 0%
where the time goes in v1:
time: 249 us; the launch traced here: 248 us
  blocking collectives  83.4 us (33%)
  matrix products  38.5 us (15%)
  starting transfers between devices  37.3 us (15%)
  local copies, waits for them, and re-layouts  33.8 us (14%)
  waiting for transfers between devices  25.2 us (10%)
  other arithmetic  16.4 us (7%)
  between operations  13.9 us (6%)
    all_to_all x1, blocking collectives, sum_at_owner(): lax.all_to_all(tiles, axis, split_axis=0, concat_axis=0, tiled=True)  83.4 us
    ppermute x7, starting transfers between devices, gather_around(): lax.ppermute(going_down, axis, [(d, (d - 1) % ways) for d in range(ways)])  35 us
    ppermute x8, waiting for transfers between devices, gather_around(): lax.ppermute(going_up, axis, [(d, (d + 1) % ways) for d in range(ways)])  20.8 us
    unnamed x13, local copies, waits for them, and re-layouts  18.2 us
    dot_general x1, matrix products, local(): jnp.dot(grad_rows.T, hidden, preferred_element_type=jnp.float32)  11.8 us
    dot_general x1, matrix products, local(): jnp.dot(pre_grad, lax.all_gather(up_weight, 'fs', axis=0, tiled=True).T,...  9.32 us
    dot_general x1, matrix products, local(): jnp.dot(columns, gather_around(down_weight, 'fs', 1).T, preferred_element...  8.99 us
    concatenate x1, other arithmetic, local(): jnp.concatenate([jnp.dot(columns.T, pre_grad, preferred_element_type=jnp....  8.48 us
  transfers between devices with their start and end apart: 18, of which 8 were waited for; matrix products, arithmetic and copies ran while one was open for 32% of the time, Pallas kernels for 0%

profile of v1, /device:TPU:1, one launch (start us, length us, event | category | flops | bytes accessed | tf_op | source)
XLA Modules:
  0.0 248.5 jit_solution(15034942445907817228)
XLA Ops:
  7.2 2.7 %pad_maximum_fusion.1 = bf16[192,4096]{1,0:T(8,128)(2,1)} fusion(bf16[192,2048]{1,0:T(8,128)(2,1)} %param.7, bf16[192,2048]{1,0:T(8,128)(2,1)} %param.5), kind=kLoop, calls=%fused_computation.14 | loop fusion | flops 3145728 | bytes 3145728 | tf_op jit(solution)/shard_map/concatenate | solution.py:30
  10.0 2.2 collective-permute-start
  12.2 5.0 %collective-permute-start.1 = (bf16[1024,128]{1,0:T(8,128)(2,1)S(1)}, bf16[1024,128]{1,0:T(8,128)(2,1)S(1)}, u32[]{:S(2)}, u32[]{:S(2)}) collective-permute-start(bf16[1024,128]{1,0:T(8,128)(2,1)S(1)} %copy-done), channel_id=1, source_target_pairs={{0,120},{8,0},{16,8},{24,16},{32,24},{40,32},{48,40},{56,48},{64,5... | collective-permute-start | bytes 786440 | tf_op jit(solution)/shard_map/ppermute | solution.py:18
  17.2 5.9 %collective-permute-done = bf16[1024,128]{1,0:T(8,128)(2,1)S(1)} collective-permute-done((bf16[1024,128]{1,0:T(8,128)(2,1)S(1)}, bf16[1024,128]{1,0:T(8,128)(2,1)S(1)}, u32[]{:S(2)}, u32[]{:S(2)}) %collective-permute-start) | collective-permute-done | bytes 262176 | tf_op jit(solution)/shard_map/ppermute | solution.py:15
  23.2 4.8 %collective-permute-start.3 = (bf16[1024,128]{1,0:T(8,128)(2,1)S(1)}, bf16[1024,128]{1,0:T(8,128)(2,1)S(1)}, u32[]{:S(2)}, u32[]{:S(2)}) collective-permute-start(bf16[1024,128]{1,0:T(8,128)(2,1)S(1)} %collective-permute-done.1), channel_id=1, source_target_pairs={{0,120},{8,0},{16,8},{24,16},{32,24},{40,32},{48,40},{56,48},{64,5... | collective-permute-start | bytes 786440 | tf_op jit(solution)/shard_map/ppermute | solution.py:18
  27.9 5.1 %collective-permute-done.2 = bf16[1024,128]{1,0:T(8,128)(2,1)S(1)} collective-permute-done((bf16[1024,128]{1,0:T(8,128)(2,1)S(1)}, bf16[1024,128]{1,0:T(8,128)(2,1)S(1)}, u32[]{:S(2)}, u32[]{:S(2)}) %collective-permute-start.2) | collective-permute-done | bytes 262176 | tf_op jit(solution)/shard_map/ppermute | solution.py:15
  33.1 4.8 %collective-permute-start.5 = (bf16[1024,128]{1,0:T(8,128)(2,1)S(1)}, bf16[1024,128]{1,0:T(8,128)(2,1)S(1)}, u32[]{:S(2)}, u32[]{:S(2)}) collective-permute-start(bf16[1024,128]{1,0:T(8,128)(2,1)S(1)} %collective-permute-done.3), channel_id=1, source_target_pairs={{0,120},{8,0},{16,8},{24,16},{32,24},{40,32},{48,40},{56,48},{64,5... | collective-permute-start | bytes 786440 | tf_op jit(solution)/shard_map/ppermute | solution.py:18
  38.0 4.2 %collective-permute-done.4 = bf16[1024,128]{1,0:T(8,128)(2,1)S(1)} collective-permute-done((bf16[1024,128]{1,0:T(8,128)(2,1)S(1)}, bf16[1024,128]{1,0:T(8,128)(2,1)S(1)}, u32[]{:S(2)}, u32[]{:S(2)}) %collective-permute-start.4) | collective-permute-done | bytes 262176 | tf_op jit(solution)/shard_map/ppermute | solution.py:15
  42.2 2.5 broadcast_in_dim.3
  46.2 4.8 %collective-permute-start.7 = (bf16[1024,128]{1,0:T(8,128)(2,1)S(1)}, bf16[1024,128]{1,0:T(8,128)(2,1)S(1)}, u32[]{:S(2)}, u32[]{:S(2)}) collective-permute-start(bf16[1024,128]{1,0:T(8,128)(2,1)S(1)} %collective-permute-done.5), channel_id=1, source_target_pairs={{0,120},{8,0},{16,8},{24,16},{32,24},{40,32},{48,40},{56,48},{64,5... | collective-permute-start | bytes 786440 | tf_op jit(solution)/shard_map/ppermute | solution.py:18
  54.3 5.2 %collective-permute-start.9 = (bf16[1024,128]{1,0:T(8,128)(2,1)S(1)}, bf16[1024,128]{1,0:T(8,128)(2,1)S(1)}, u32[]{:S(2)}, u32[]{:S(2)}) collective-permute-start(bf16[1024,128]{1,0:T(8,128)(2,1)S(1)} %collective-permute-done.7), channel_id=1, source_target_pairs={{0,120},{8,0},{16,8},{24,16},{32,24},{40,32},{48,40},{56,48},{64,5... | collective-permute-start | bytes 786440 | tf_op jit(solution)/shard_map/ppermute | solution.py:18
  62.8 5.2 %collective-permute-start.11 = (bf16[1024,128]{1,0:T(8,128)(2,1)S(1)}, bf16[1024,128]{1,0:T(8,128)(2,1)S(1)}, u32[]{:S(2)}, u32[]{:S(2)}) collective-permute-start(bf16[1024,128]{1,0:T(8,128)(2,1)S(1)} %collective-permute-done.9), channel_id=1, source_target_pairs={{0,120},{8,0},{16,8},{24,16},{32,24},{40,32},{48,40},{56,48},{64,5... | collective-permute-start | bytes 786440 | tf_op jit(solution)/shard_map/ppermute | solution.py:18
  71.3 5.2 %collective-permute-start.13 = (bf16[1024,128]{1,0:T(8,128)(2,1)S(1)}, bf16[1024,128]{1,0:T(8,128)(2,1)S(1)}, u32[]{:S(2)}, u32[]{:S(2)}) collective-permute-start(bf16[1024,128]{1,0:T(8,128)(2,1)S(1)} %collective-permute-done.11), channel_id=1, source_target_pairs={{0,120},{8,0},{16,8},{24,16},{32,24},{40,32},{48,40},{56,48},{64,5... | collective-permute-start | bytes 786440 | tf_op jit(solution)/shard_map/ppermute | solution.py:18
  80.9 5.5 %collective-permute-done.14 = bf16[1024,128]{1,0:T(8,128)(2,1)S(1)} collective-permute-done((bf16[1024,128]{1,0:T(8,128)(2,1)S(1)}, bf16[1024,128]{1,0:T(8,128)(2,1)S(1)}, u32[]{:S(2)}, u32[]{:S(2)}) %collective-permute-start.14) | collective-permute-done | bytes 262176 | tf_op jit(solution)/shard_map/ppermute | solution.py:15
  87.3 11.8 %fusion.8 = bf16[2048,1024]{0,1:T(8,128)(2,1)} fusion(bf16[1536,4096]{1,0:T(8,128)(2,1)} %all-gather.3.cloned.1.call-done, bf16[1536,1024]{1,0:T(8,128)(2,1)} %param.6), kind=kOutput, calls=%fused_computation.11 | convolution fusion | flops 6450839552 | bytes 13631488 | tf_op jit(solution)/shard_map/dot_general | solution.py:68
  99.1 9.0 %multiply_convert_fusion.1 = bf16[1536,1024]{1,0:T(8,128)(2,1)S(1)} fusion(bf16[1536,1024]{1,0:T(8,128)(2,1)S(1)} %copy-done.2, bf16[1024,2048]{1,0:T(8,128)(2,1)} %constant_dynamic-update-slice_fusion, bf16[1536,4096]{1,0:T(8,128)(2,1)S(1)} %copy-done.1), kind=kOutput, calls=%fused_computation.5 | convolution fusion | flops 6450315264 | bytes 16777216 | tf_op jit(solution)/shard_map/dot_general | solution.py:51
  108.1 1.7 copy-done.3
  109.8 8.4 %fusion.11 = bf16[2048,1024]{0,1:T(8,128)(2,1)} fusion(bf16[1536,1024]{1,0:T(8,128)(2,1)S(1)} %multiply_convert_fusion.1, bf16[1536,4096]{1,0:T(8,128)(2,1)S(1)} %copy-done.1), kind=kOutput, calls=%fused_computation.12 | convolution fusion | flops 6444548096 | bytes 13631488 | tf_op jit(solution)/shard_map/dot_general | solution.py:67
  118.1 8.5 %pad_maximum_fusion = bf16[2048,2048]{0,1:T(8,128)(2,1)} fusion(bf16[2048,1024]{0,1:T(8,128)(2,1)} %fusion.8, bf16[2048,1024]{0,1:T(8,128)(2,1)} %fusion.11), kind=kLoop, calls=%fused_computation | loop fusion | flops 16777216 | bytes 16777216 | tf_op jit(solution)/shard_map/concatenate | solution.py:65
  126.6 12.4 %copy.10 = bf16[2048,2048]{1,0:T(8,128)(2,1)} copy(bf16[2048,2048]{0,1:T(8,128)(2,1)} %pad_maximum_fusion) | data formatting | bytes 16777216
  139.0 1.8 copy-done.4
  140.9 9.3 %convolution_convert_fusion = bf16[1536,2048]{1,0:T(8,128)(2,1)S(1)} fusion(bf16[1536,1024]{1,0:T(8,128)(2,1)S(1)} %copy-done.4, bf16[2048,1024]{1,0:T(8,128)(2,1)} %all-gather.5.cloned.1.call-done), kind=kOutput, calls=%fused_computation.1 | convolution fusion | flops 6445596672 | bytes 13631488 | tf_op jit(solution)/shard_map/dot_general | solution.py:55
  150.2 83.4 %all_to_all.5 = bf16[8,192,2048]{2,1,0:T(8,128)(2,1)} all-to-all(bf16[8,192,2048]{2,1,0:T(8,128)(2,1)S(1)} %bitcast.8), channel_id=1, replica_groups=mesh['fs'=16,'tp'=8] {'tp'}, dimensions={0} | all-to-all | bytes 12582912 | tf_op jit(solution)/shard_map/all_to_all | solution.py:41
  233.6 5.1 %reduce_sum.12 = bf16[192,2048]{1,0:T(8,128)(2,1)} reduce(bf16[8,192,2048]{2,1,0:T(8,128)(2,1)} %all_to_all.5, bf16[]{:T(256)} %constant.96.clone.1), dimensions={0}, to_apply=%region_0.1 | reduce | flops 2752512 | bytes 7077890 | tf_op jit(solution)/shard_map/reduce_sum | solution.py:42
  (56 shorter events, 20.1 us)
Async XLA Ops:
  7.2 2.9 %copy-start = (bf16[1024,128]{1,0:T(8,128)(2,1)S(1)}, bf16[1024,128]{1,0:T(8,128)(2,1)}, u32[]{:S(2)}) copy-start(bf16[1024,128]{1,0:T(8,128)(2,1)} %param.9) | copy-start | bytes 786436
  7.2 80.1 %all-gather.3.cloned.1.call-start = ((), (), s32[]{:S(2)}) async-start(), calls=%async_computation.2 | async-start | bytes 14155776 | tf_op jit(solution)/shard_map/all_gather | solution.py:31
  10.0 129.0 %all-gather.5.cloned.1.call-start = ((), (), s32[]{:S(2)}) async-start(), calls=%async_computation.3 | async-start | bytes 4456448 | tf_op jit(solution)/shard_map/all_gather | solution.py:57
  10.0 13.1 %collective-permute-start = (bf16[1024,128]{1,0:T(8,128)(2,1)S(1)}, bf16[1024,128]{1,0:T(8,128)(2,1)S(1)}, u32[]{:S(2)}, u32[]{:S(2)}) collective-permute-start(bf16[1024,128]{1,0:T(8,128)(2,1)S(1)} %copy-done), channel_id=1, source_target_pairs={{0,8},{8,16},{16,24},{24,32},{32,40},{40,48},{48,56},{56,64},{64,7... | collective-permute-start | bytes 786440 | tf_op jit(solution)/shard_map/ppermute | solution.py:15
  12.2 10.9 %collective-permute-start.1 = (bf16[1024,128]{1,0:T(8,128)(2,1)S(1)}, bf16[1024,128]{1,0:T(8,128)(2,1)S(1)}, u32[]{:S(2)}, u32[]{:S(2)}) collective-permute-start(bf16[1024,128]{1,0:T(8,128)(2,1)S(1)} %copy-done), channel_id=1, source_target_pairs={{0,120},{8,0},{16,8},{24,16},{32,24},{40,32},{48,40},{56,48},{64,5... | collective-permute-start | bytes 786440 | tf_op jit(solution)/shard_map/ppermute | solution.py:18
  23.2 9.9 %collective-permute-start.2 = (bf16[1024,128]{1,0:T(8,128)(2,1)S(1)}, bf16[1024,128]{1,0:T(8,128)(2,1)S(1)}, u32[]{:S(2)}, u32[]{:S(2)}) collective-permute-start(bf16[1024,128]{1,0:T(8,128)(2,1)S(1)} %collective-permute-done), channel_id=1, source_target_pairs={{0,8},{8,16},{16,24},{24,32},{32,40},{40,48},{48,56},{56,64},{64,7... | collective-permute-start | bytes 786440 | tf_op jit(solution)/shard_map/ppermute | solution.py:15
  23.2 9.9 %collective-permute-start.3 = (bf16[1024,128]{1,0:T(8,128)(2,1)S(1)}, bf16[1024,128]{1,0:T(8,128)(2,1)S(1)}, u32[]{:S(2)}, u32[]{:S(2)}) collective-permute-start(bf16[1024,128]{1,0:T(8,128)(2,1)S(1)} %collective-permute-done.1), channel_id=1, source_target_pairs={{0,120},{8,0},{16,8},{24,16},{32,24},{40,32},{48,40},{56,48},{64,5... | collective-permute-start | bytes 786440 | tf_op jit(solution)/shard_map/ppermute | solution.py:18
  33.1 9.1 %collective-permute-start.4 = (bf16[1024,128]{1,0:T(8,128)(2,1)S(1)}, bf16[1024,128]{1,0:T(8,128)(2,1)S(1)}, u32[]{:S(2)}, u32[]{:S(2)}) collective-permute-start(bf16[1024,128]{1,0:T(8,128)(2,1)S(1)} %collective-permute-done.2), channel_id=1, source_target_pairs={{0,8},{8,16},{16,24},{24,32},{32,40},{40,48},{48,56},{56,64},{64,7... | collective-permute-start | bytes 786440 | tf_op jit(solution)/shard_map/ppermute | solution.py:15
  33.1 13.1 %collective-permute-start.5 = (bf16[1024,128]{1,0:T(8,128)(2,1)S(1)}, bf16[1024,128]{1,0:T(8,128)(2,1)S(1)}, u32[]{:S(2)}, u32[]{:S(2)}) collective-permute-start(bf16[1024,128]{1,0:T(8,128)(2,1)S(1)} %collective-permute-done.3), channel_id=1, source_target_pairs={{0,120},{8,0},{16,8},{24,16},{32,24},{40,32},{48,40},{56,48},{64,5... | collective-permute-start | bytes 786440 | tf_op jit(solution)/shard_map/ppermute | solution.py:18
  37.9 200.8 %reduce-scatter.4.cloned.1.call-start = ((), (), s32[]{:S(2)}) async-start(), calls=%async_computation.4 | async-start | bytes 8912896
  42.2 9.5 %collective-permute-start.6 = (bf16[1024,128]{1,0:T(8,128)(2,1)S(1)}, bf16[1024,128]{1,0:T(8,128)(2,1)S(1)}, u32[]{:S(2)}, u32[]{:S(2)}) collective-permute-start(bf16[1024,128]{1,0:T(8,128)(2,1)S(1)} %collective-permute-done.4), channel_id=1, source_target_pairs={{0,8},{8,16},{16,24},{24,32},{32,40},{40,48},{48,56},{56,64},{64,7... | collective-permute-start | bytes 786440 | tf_op jit(solution)/shard_map/ppermute | solution.py:15
  46.2 8.1 %collective-permute-start.7 = (bf16[1024,128]{1,0:T(8,128)(2,1)S(1)}, bf16[1024,128]{1,0:T(8,128)(2,1)S(1)}, u32[]{:S(2)}, u32[]{:S(2)}) collective-permute-start(bf16[1024,128]{1,0:T(8,128)(2,1)S(1)} %collective-permute-done.5), channel_id=1, source_target_pairs={{0,120},{8,0},{16,8},{24,16},{32,24},{40,32},{48,40},{56,48},{64,5... | collective-permute-start | bytes 786440 | tf_op jit(solution)/shard_map/ppermute | solution.py:18
  51.7 8.6 %collective-permute-start.8 = (bf16[1024,128]{1,0:T(8,128)(2,1)S(1)}, bf16[1024,128]{1,0:T(8,128)(2,1)S(1)}, u32[]{:S(2)}, u32[]{:S(2)}) collective-permute-start(bf16[1024,128]{1,0:T(8,128)(2,1)S(1)} %collective-permute-done.6), channel_id=1, source_target_pairs={{0,8},{8,16},{16,24},{24,32},{32,40},{40,48},{48,56},{56,64},{64,7... | collective-permute-start | bytes 786440 | tf_op jit(solution)/shard_map/ppermute | solution.py:15
  54.3 8.5 %collective-permute-start.9 = (bf16[1024,128]{1,0:T(8,128)(2,1)S(1)}, bf16[1024,128]{1,0:T(8,128)(2,1)S(1)}, u32[]{:S(2)}, u32[]{:S(2)}) collective-permute-start(bf16[1024,128]{1,0:T(8,128)(2,1)S(1)} %collective-permute-done.7), channel_id=1, source_target_pairs={{0,120},{8,0},{16,8},{24,16},{32,24},{40,32},{48,40},{56,48},{64,5... | collective-permute-start | bytes 786440 | tf_op jit(solution)/shard_map/ppermute | solution.py:18
  60.3 8.5 %collective-permute-start.10 = (bf16[1024,128]{1,0:T(8,128)(2,1)S(1)}, bf16[1024,128]{1,0:T(8,128)(2,1)S(1)}, u32[]{:S(2)}, u32[]{:S(2)}) collective-permute-start(bf16[1024,128]{1,0:T(8,128)(2,1)S(1)} %collective-permute-done.8), channel_id=1, source_target_pairs={{0,8},{8,16},{16,24},{24,32},{32,40},{40,48},{48,56},{56,64},{64,7... | collective-permute-start | bytes 786440 | tf_op jit(solution)/shard_map/ppermute | solution.py:15
  62.8 8.5 %collective-permute-start.11 = (bf16[1024,128]{1,0:T(8,128)(2,1)S(1)}, bf16[1024,128]{1,0:T(8,128)(2,1)S(1)}, u32[]{:S(2)}, u32[]{:S(2)}) collective-permute-start(bf16[1024,128]{1,0:T(8,128)(2,1)S(1)} %collective-permute-done.9), channel_id=1, source_target_pairs={{0,120},{8,0},{16,8},{24,16},{32,24},{40,32},{48,40},{56,48},{64,5... | collective-permute-start | bytes 786440 | tf_op jit(solution)/shard_map/ppermute | solution.py:18
  68.8 8.5 %collective-permute-start.12 = (bf16[1024,128]{1,0:T(8,128)(2,1)S(1)}, bf16[1024,128]{1,0:T(8,128)(2,1)S(1)}, u32[]{:S(2)}, u32[]{:S(2)}) collective-permute-start(bf16[1024,128]{1,0:T(8,128)(2,1)S(1)} %collective-permute-done.10), channel_id=1, source_target_pairs={{0,8},{8,16},{16,24},{24,32},{32,40},{40,48},{48,56},{56,64},{64,7... | collective-permute-start | bytes 786440 | tf_op jit(solution)/shard_map/ppermute | solution.py:15
  71.3 8.8 %collective-permute-start.13 = (bf16[1024,128]{1,0:T(8,128)(2,1)S(1)}, bf16[1024,128]{1,0:T(8,128)(2,1)S(1)}, u32[]{:S(2)}, u32[]{:S(2)}) collective-permute-start(bf16[1024,128]{1,0:T(8,128)(2,1)S(1)} %collective-permute-done.11), channel_id=1, source_target_pairs={{0,120},{8,0},{16,8},{24,16},{32,24},{40,32},{48,40},{56,48},{64,5... | collective-permute-start | bytes 786440 | tf_op jit(solution)/shard_map/ppermute | solution.py:18
  77.4 9.1 %collective-permute-start.14 = (bf16[1024,128]{1,0:T(8,128)(2,1)S(1)}, bf16[1024,128]{1,0:T(8,128)(2,1)S(1)}, u32[]{:S(2)}, u32[]{:S(2)}) collective-permute-start(bf16[1024,128]{1,0:T(8,128)(2,1)S(1)} %collective-permute-done.12), channel_id=1, source_target_pairs={{0,8},{8,16},{16,24},{24,32},{32,40},{40,48},{48,56},{56,64},{64,7... | collective-permute-start | bytes 786440 | tf_op jit(solution)/shard_map/ppermute | solution.py:15
  87.2 11.8 %copy-start.2 = (bf16[1536,1024]{1,0:T(8,128)(2,1)S(1)}, bf16[1536,1024]{1,0:T(8,128)(2,1)}, u32[]{:S(2)}) copy-start(bf16[1536,1024]{1,0:T(8,128)(2,1)} %param.6) | copy-start | bytes 9437188
  87.2 11.8 %copy-start.1 = (bf16[1536,4096]{1,0:T(8,128)(2,1)S(1)}, bf16[1536,4096]{1,0:T(8,128)(2,1)}, u32[]{:S(2)}) copy-start(bf16[1536,4096]{1,0:T(8,128)(2,1)} %all-gather.3.cloned.1.call-done) | copy-start | bytes 37748740
  108.1 1.7 copy-start.3
  139.0 1.9 copy-start.4
Sparse Core Ops, SparseCore 0:
  10.1 70.8 all-gather.2
  83.1 51.3 all-gather.4
  139.1 88.4 reduce-scatter.3
